TPU v7x, 32 devices: a whole 2x2x4 slice. The times are simulated.
32 devices in a mesh: grp: 2 (over y), fs: 4 (over z), tp: 4 (over x, core).
Axes of the slice: x: 2, y: 2, z: 4, core: 2. Of those that a mesh axis runs over, the one named last changes fastest.
Arguments:
- tokens: bfloat16 [8192, 2048], P(('grp', 'fs', 'tp')), parts along dimension 0, may hold values from -6 to 6
- norm_gains: float32 [4, 2048], replicated, may hold values from 0.1 to 1.9
- query_weight: bfloat16 [2048, 2048], P('fs', 'tp'), may hold values from -0.125 to 0.125
- key_weight: bfloat16 [2048, 2048], P('fs', 'tp'), may hold values from -0.125 to 0.125
- value_weight: bfloat16 [2048, 4096], P('fs', 'tp'), may hold values from -0.125 to 0.125
- swish_weight: bfloat16 [2048, 4096], P('fs', 'tp'), may hold values from -0.125 to 0.125
- mixer_output: bfloat16 [4096, 2048], P('tp', 'fs'), may hold values from -0.09375 to 0.09375
- gate_weight: bfloat16 [2048, 3072], P('fs', 'tp'), may hold values from -0.125 to 0.125
- up_weight: bfloat16 [2048, 3072], P('fs', 'tp'), may hold values from -0.125 to 0.125
- down_weight: bfloat16 [3072, 2048], P('tp', 'fs'), may hold values from -0.109375 to 0.109375
Outputs:
- layer_output: bfloat16 [8192, 2048], P(('grp', 'fs', 'tp')), parts along dimension 0
There are 2 independent parts, one for each index of `grp`. A program takes and returns all parts, laid end to end along the dimension named above; an argument that names none is the same for every part. Nothing has to cross between parts.
All inputs are finite; a program needn't handle non-finite values.
Results may differ from a plain program's by a relative error of at most 0.02.
Values may be sent and summed in bfloat16 or wider, within the bound.
A program may use at most 128 MiB of HBM per device.

v0:
```python
import functools
import math

import jax
import jax.numpy as jnp
from jax import lax
from jax.experimental import pallas as pl
from jax.experimental.pallas import tpu as pltpu
from jax.sharding import PartitionSpec as P

QK = 256
BLOCK = 128
CORES = 2

norm_epsilon = 1e-06
group_epsilon = 0.01

MESH = pl.DeviceIdType.MESH
f32, bf16 = jnp.float32, jnp.bfloat16

WQ, WK, WV, WS, WM, WG, WU, WD = range(8)


def rms(matrix):
    return matrix * lax.rsqrt(jnp.mean(matrix * matrix, axis=-1, keepdims=True) + norm_epsilon)


def silu(value):
    return value / (1.0 + jnp.exp(-value))


def dot(left, right):
    return jnp.dot(left, right, preferred_element_type=f32)


def ds(start, size, multiple=None):
    return pl.ds(pl.multiple_of(start, multiple or size), size)


def layer(G, F, T, *refs):
    tokens, gains, cosine, sine = refs[:4]
    shards = refs[4:12]
    out = refs[12]
    bufs = refs[13:21]
    (act, queries, keys, values, swish, gated, after, total, send1, recv1, send2, recv2) = refs[21:33]
    (local_sem, z_send, z_recv, y_send, y_recv, ag_x_send, ag_x_recv, ag_c_send, ag_c_recv,
     rs1_send, rs1_recv, rs2_send, rs2_recv) = refs[33:]

    X = T // CORES
    g, f, t = lax.axis_index("grp"), lax.axis_index("fs"), lax.axis_index("tp")
    x, c = t // CORES, t % CORES
    R, D = tokens.shape
    L = R * T
    TM = min(256, L)
    heads = queries.shape[1] // QK
    VD = values.shape[1] // heads
    FH = bufs[WG].shape[1]
    partner = (g, f, x * CORES + (1 - c))

    def x_peer(o):
        return lax.rem(x + o, X)

    neighbours = [(f > 0, (g, f - 1, t)), (f < F - 1, (g, f + 1, t))]
    neighbours += [(None, (lax.rem(g + o, G), f, t)) for o in range(1, G)]
    neighbours += [(None, (g, f, x_peer(o) * CORES + c)) for o in range(1, X)]
    neighbours += [(None, partner)]

    def when(condition, action):
        if condition is None:
            action()
        else:
            pl.when(condition)(action)

    def local_copy(w):
        r = shards[w].shape[0]
        return pltpu.make_async_copy(shards[w], bufs[w].at[ds(f * r, r)], local_sem.at[w])

    def half(w, s, part):
        r = shards[w].shape[0]
        return bufs[w].at[ds(s * r + part * (r // G), r // G)]

    def source(d, k):
        return (f - k if d == 0 else f + k)

    def valid(d, k):
        return (f >= k if d == 0 else f + k < F)

    def z_copy(w, k, d):
        region = half(w, source(d, k), g)
        return pltpu.make_async_remote_copy(
            region, region, z_send.at[d, w, k], z_recv.at[d, w, k + 1],
            device_id=(g, f + 1 if d == 0 else f - 1, t), device_id_type=MESH)

    def z_wait(w, k, d):
        region = half(w, source(d, k), g)
        pltpu.make_async_remote_copy(
            region, region, z_send.at[d, w, k], z_recv.at[d, w, k],
            device_id=(g, f, t), device_id_type=MESH).wait_recv()

    def y_copy(w, k, d, o):
        region = half(w, source(d, k), g)
        return pltpu.make_async_remote_copy(
            region, region, y_send.at[d, w, k, o], y_recv.at[d, w, k, o],
            device_id=(lax.rem(g + o, G), f, t), device_id_type=MESH)

    def y_wait(w, k, d, o):
        region = half(w, source(d, k), lax.rem(g + G - o, G))
        pltpu.make_async_remote_copy(
            region, region, y_send.at[d, w, k, o], y_recv.at[d, w, k, o],
            device_id=(g, f, t), device_id_type=MESH).wait_recv()

    def has_next(d):
        return f < F - 1 if d == 0 else f > 0

    def comm(w, k):
        if k == 0:
            local_copy(w).wait()
        for d in range(2):
            if k == 0:
                pl.when(has_next(d))(lambda d=d: z_copy(w, k, d).start())
            else:
                @pl.when(valid(d, k))
                def _(d=d):
                    z_wait(w, k, d)
                    if k < F - 1:
                        pl.when(has_next(d))(lambda: z_copy(w, k, d).start())
                    for o in range(1, G):
                        y_copy(w, k, d, o).start()

    def arrived(w):
        for k in range(1, F):
            for d in range(2):
                @pl.when(valid(d, k))
                def _(k=k, d=d):
                    for o in range(1, G):
                        y_wait(w, k, d, o)

    def drain(w):
        for k in range(F):
            for d in range(2):
                @pl.when(valid(d, k))
                def _(k=k, d=d):
                    if k < F - 1:
                        pl.when(has_next(d))(lambda: z_copy(w, k, d).wait_send())
                    if k > 0:
                        for o in range(1, G):
                            y_copy(w, k, d, o).wait_send()

    def rows_of(device):
        return act.at[ds(device * R, R)]

    def ag_x(stage, o):
        region = rows_of(t)
        return pltpu.make_async_remote_copy(
            region, region, ag_x_send.at[stage, o], ag_x_recv.at[stage, o],
            device_id=(g, f, x_peer(o) * CORES + c), device_id_type=MESH)

    def ag_c(stage, o, core):
        region = rows_of(x_peer(X - o) * CORES + core)
        return pltpu.make_async_remote_copy(
            region, region, ag_c_send.at[stage, o], ag_c_recv.at[stage, o],
            device_id=partner, device_id_type=MESH)

    def gather_start(stage):
        for o in range(1, X):
            ag_x(stage, o).start()
        ag_c(stage, 0, c).start()

    def gather_forward(stage):
        for o in range(1, X):
            region = rows_of(x_peer(X - o) * CORES + c)
            pltpu.make_async_remote_copy(
                region, region, ag_x_send.at[stage, o], ag_x_recv.at[stage, o],
                device_id=(g, f, t), device_id_type=MESH).wait_recv()
            ag_c(stage, o, c).start()

    def gather_wait(stage):
        for o in range(X):
            ag_c(stage, o, 1 - c).wait_recv()

    def gather_drain(stage):
        for o in range(X):
            if o:
                ag_x(stage, o).wait_send()
            ag_c(stage, o, c).wait_send()

    def rs1(stage, j):
        return pltpu.make_async_remote_copy(
            send1.at[j], recv1.at[j], rs1_send.at[stage, j], rs1_recv.at[stage, j],
            device_id=partner, device_id_type=MESH)

    def rs2(stage, j, o):
        return pltpu.make_async_remote_copy(
            send2.at[j, o], recv2.at[j, o], rs2_send.at[stage, j, o], rs2_recv.at[stage, j, o],
            device_id=(g, f, x_peer(o) * CORES + c), device_id_type=MESH)

    def partial_rows(w, width, j, device):
        r = shards[w].shape[0]
        return dot(gated[ds(device * R, R), :width], bufs[w][ds(j * r, r), :])

    def sum_send(stage, w, width, j):
        def one(o, _):
            send1[j, o] = partial_rows(w, width, j, o * CORES + (1 - c)).astype(bf16)
            return 0
        lax.fori_loop(0, X, one, 0)
        rs1(stage, j).start()

    def sum_pass(stage, w, width, j):
        cols = send1.shape[-1]
        rs1(stage, j).wait_recv()
        def pair(o):
            peer = x_peer(o)
            return partial_rows(w, width, j, peer * CORES + c) + recv1[j, peer].astype(f32)
        for o in range(1, X):
            send2[j, o] = pair(o).astype(bf16)
            rs2(stage, j, o).start()
        total[:, ds(j * cols, cols)] = pair(0)

    def sum_finish(stage):
        cols = send1.shape[-1]
        def one(j, _):
            for o in range(1, X):
                rs2(stage, j, o).wait_recv()
                total[:, ds(j * cols, cols)] += recv2[j, o].astype(f32)
            return 0
        lax.fori_loop(0, F, one, 0)

    def sum_drain(stage):
        def one(j, _):
            rs1(stage, j).wait_send()
            for o in range(1, X):
                rs2(stage, j, o).wait_send()
            return 0
        lax.fori_loop(0, F, one, 0)

    RT = min(32, R)

    def norm_in():
        def one(i, _):
            rows = ds(i * RT, RT)
            act[ds(t * R + i * RT, RT)] = (
                rms(tokens[rows].astype(f32)) * gains[0:1]).astype(bf16)
            return 0
        lax.fori_loop(0, R // RT, one, 0)

    def norm_mid():
        def one(i, _):
            rows = ds(i * RT, RT)
            mid = tokens[rows].astype(f32) + rms(total[rows]) * gains[1:2]
            after[rows] = mid
            act[ds(t * R + i * RT, RT)] = (rms(mid) * gains[2:3]).astype(bf16)
            return 0
        lax.fori_loop(0, R // RT, one, 0)

    def norm_out():
        def one(i, _):
            rows = ds(i * RT, RT)
            out[rows] = (after[rows] + rms(total[rows]) * gains[3:4]).astype(bf16)
            return 0
        lax.fori_loop(0, R // RT, one, 0)

    def tiles(width, tile, body):
        across = width // tile

        def one(i, _):
            body(ds((i // across) * TM, TM), ds((i % across) * tile, tile))
            return 0
        lax.fori_loop(0, (L // TM) * across, one, 0)

    def rotary(w, into, scale):
        def body(rows, cols):
            head = dot(act[rows], bufs[w][:, cols])
            lower, upper = head[:, :QK // 2], head[:, QK // 2:]
            cos, sin = cosine[rows], sine[rows]
            rotated = jnp.concatenate(
                [lower * cos - upper * sin, lower * sin + upper * cos], axis=-1)
            into[rows, cols] = (rotated * scale).astype(bf16)
        tiles(heads * QK, QK, body)

    def project(w, into):
        def body(rows, cols):
            into[rows, cols] = dot(act[rows], bufs[w][:, cols]).astype(into.dtype)
        tiles(heads * VD, VD, body)

    def retain(h):
        head_index = (t * heads + h).astype(f32)
        fraction = jnp.full((1, 1), 1.0, f32) * (head_index / (heads * T - 1.0))
        log_decay = -(4.0 / BLOCK) * jnp.exp(fraction * math.log(BLOCK / (32.0 * L)))
        qk_cols = ds(h * QK, QK)
        v_cols = ds(h * VD, VD)
        for i in range(L // TM):
            rows, seen = pl.ds(i * TM, TM), (i + 1) * TM
            scores = lax.dot_general(
                queries[rows, qk_cols], keys[:seen, qk_cols], (((1,), (1,)), ((), ())),
                preferred_element_type=f32)
            distance = (lax.broadcasted_iota(jnp.int32, (TM, seen), 0) + i * TM
                        - lax.broadcasted_iota(jnp.int32, (TM, seen), 1)).astype(f32)
            weights = jnp.where(
                distance >= 0, jnp.exp(log_decay * jnp.maximum(distance, 0.0)), 0.0)
            retained = dot((scores * weights).astype(bf16), values[:seen, v_cols])
            centred = retained - jnp.mean(retained, axis=-1, keepdims=True)
            normalized = centred * lax.rsqrt(
                jnp.mean(centred * centred, axis=-1, keepdims=True) + group_epsilon)
            gated[rows, v_cols] = (silu(swish[rows, v_cols]) * normalized).astype(bf16)

    def hidden_units():
        def body(rows, cols):
            up = dot(act[rows], bufs[WU][:, cols])
            gate = dot(act[rows], bufs[WG][:, cols])
            gated[rows, cols] = (silu(gate) * up).astype(bf16)
        tiles(FH, math.gcd(FH, 256), body)

    for w in range(8):
        local_copy(w).start()
    barrier = pltpu.get_barrier_semaphore()
    for condition, device in neighbours:
        when(condition, lambda device=device: pl.semaphore_signal(
            barrier, inc=1, device_id=device, device_id_type=MESH))
    fixed = (G - 1) + (X - 1) + 1
    pl.semaphore_wait(
        barrier, fixed + (f > 0).astype(jnp.int32) + (f < F - 1).astype(jnp.int32))

    comm(WQ, 0)
    comm(WK, 0)
    norm_in()
    gather_start(0)
    for k in range(1, F):
        comm(WQ, k)
    comm(WV, 0)
    comm(WK, 1)
    gather_forward(0)
    for k in range(2, F):
        comm(WK, k)
    comm(WS, 0)
    gather_wait(0)
    arrived(WQ)
    rotary(WQ, queries, 1.0)
    comm(WV, 1)
    arrived(WK)
    rotary(WK, keys, QK ** -0.5)
    for k in range(2, F):
        comm(WV, k)
    comm(WM, 0)
    comm(WS, 1)
    arrived(WV)
    project(WV, values)
    for k in range(2, F):
        comm(WS, k)
    comm(WG, 0)
    comm(WM, 1)
    arrived(WS)
    project(WS, swish)
    gather_drain(0)
    if F > 2:
        comm(WM, 2)
    lax.fori_loop(0, heads, lambda h, _: (retain(h), 0)[1], 0)
    for k in range(3, F):
        comm(WM, k)
    comm(WU, 0)
    arrived(WM)

    def mixer(j, _):
        pl.when(j < F)(lambda: sum_send(0, WM, heads * VD, jnp.minimum(j, F - 1)))
        pl.when(j > 0)(lambda: sum_pass(0, WM, heads * VD, jnp.maximum(j - 1, 0)))
        return 0
    lax.fori_loop(0, F + 1, mixer, 0)
    for k in range(1, F):
        comm(WG, k)
    comm(WD, 0)
    sum_finish(0)
    norm_mid()
    gather_start(1)
    for k in range(1, F):
        comm(WU, k)
    gather_forward(1)
    comm(WD, 1)
    gather_wait(1)
    arrived(WG)
    arrived(WU)
    sum_drain(0)
    hidden_units()

    def down(j, first, second):
        if first:
            sum_send(1, WD, FH, j)
        if second:
            sum_pass(1, WD, FH, j)
    down(f, True, True)
    for k in range(1, F):
        if k > 1:
            comm(WD, k)
        for d in range(2):
            @pl.when(valid(d, k))
            def _(k=k, d=d):
                for o in range(1, G):
                    y_wait(WD, k, d, o)
                sum_send(1, WD, FH, source(d, k))
                sum_pass(1, WD, FH, source(d, k))
    sum_finish(1)
    norm_out()
    gather_drain(1)
    sum_drain(1)
    for w in range(8):
        drain(w)


def per_device(tokens, norm_gains, *weights):
    G, F, T = lax.axis_size("grp"), lax.axis_size("fs"), lax.axis_size("tp")
    X = T // CORES
    R, D = tokens.shape
    L = R * T
    query, _, value, _, mixer, gate, _, down = weights
    qk_width, v_width, hidden = query.shape[1], value.shape[1], gate.shape[1]
    positions = jnp.arange(L, dtype=f32)
    frequency = 10000.0 ** (-jnp.linspace(0.0, 1.0, QK // 2, dtype=f32))
    angles = positions[:, None] * frequency[None, :]
    vmem = pl.BlockSpec(memory_space=pltpu.VMEM)
    anywhere = pl.BlockSpec(memory_space=pl.ANY)
    DMA = pltpu.SemaphoreType.DMA
    cols = mixer.shape[1]
    scratch = [pltpu.VMEM((w.shape[0] * F, w.shape[1]), bf16) for w in weights]
    scratch += [
        pltpu.VMEM((L, D), bf16),
        pltpu.VMEM((L, qk_width), bf16),
        pltpu.VMEM((L, qk_width), bf16),
        pltpu.VMEM((L, v_width), bf16),
        pltpu.VMEM((L, v_width), f32),
        pltpu.VMEM((L, max(v_width, hidden)), bf16),
        pltpu.VMEM((R, D), f32),
        pltpu.VMEM((R, D), f32),
        pltpu.VMEM((F, X, R, cols), bf16),
        pltpu.VMEM((F, X, R, cols), bf16),
        pltpu.VMEM((F, X, R, cols), bf16),
        pltpu.VMEM((F, X, R, cols), bf16),
        DMA((8,)),
        DMA((2, 8, F)), DMA((2, 8, F)), DMA((2, 8, F, G)), DMA((2, 8, F, G)),
        DMA((2, X)), DMA((2, X)), DMA((2, X)), DMA((2, X)),
        DMA((2, F)), DMA((2, F)), DMA((2, F, X)), DMA((2, F, X)),
    ]
    return pl.pallas_call(
        functools.partial(layer, G, F, T),
        out_shape=jax.ShapeDtypeStruct((R, D), bf16),
        in_specs=[vmem] * 4 + [anywhere] * 8,
        out_specs=vmem,
        scratch_shapes=scratch,
        compiler_params=pltpu.CompilerParams(
            collective_id=0, has_side_effects=True, vmem_limit_bytes=67043328),
    )(tokens, norm_gains, jnp.cos(angles), jnp.sin(angles), *weights)


def solution(mesh):
    placed = (
        P(("grp", "fs", "tp"), None),
        P(),
        P("fs", "tp"),
        P("fs", "tp"),
        P("fs", "tp"),
        P("fs", "tp"),
        P("tp", "fs"),
        P("fs", "tp"),
        P("fs", "tp"),
        P("tp", "fs"),
    )
    return jax.shard_map(
        per_device,
        mesh=mesh,
        in_specs=placed,
        out_specs=P(("grp", "fs", "tp"), None),
        check_vma=False,
    )
```

profile of v0, /device:TPU:24, one launch (start us, length us, event | category | flops | bytes accessed | tf_op | source)
XLA Modules:
  0.0 281.7 jit_solution(3002941642254722911)
XLA Ops:
  0.0 0.1 fusion.2
  0.1 2.8 fusion
  2.9 276.5 %shard_map.100 = bf16[256,2048]{1,0:T(8,128)(2,1)} custom-call(bf16[256,2048]{1,0:T(8,128)(2,1)} %refs_0_.1, f32[4,2048]{1,0:T(4,128)} %refs_1_.1, f32[1024,128]{1,0:T(8,128)} %get-tuple-element.6.refs_2_, f32[1024,128]{1,0:T(8,128)} %get-tuple-element.5.refs_3_, bf16[512,512]{1,0:T(8,128)(2,1)} %refs_4_.1, bf16[512,512]{1,0:T(8,128)(2,1)} %refs_5_.1, ...), custom_call_target="tpu_custom_call" | custom-call | tf_op jit(solution)/shard_map/pallas_call | solution.py:440
  279.4 2.3 copy.12
  (1 shorter events, 0.0 us)
where the time goes:
time: 286 us; the launch traced here: 282 us
  Pallas kernels  276 us (97%)
  other arithmetic  2.9 us (1%)
    pallas_call x1, Pallas kernels, per_device(): pl.pallas_call(functools.partial(layer, G, F, T), out_shape=jax.ShapeDtyp...  276 us

commit v1 on v0

v1 whole, which is shorter than its diff:
```python
import functools
import math

import jax
import jax.numpy as jnp
from jax import lax
from jax.experimental import pallas as pl
from jax.experimental.pallas import tpu as pltpu
from jax.sharding import PartitionSpec as P

QK = 256
BLOCK = 128
CORES = 2

norm_epsilon = 1e-06
group_epsilon = 0.01

MESH = pl.DeviceIdType.MESH
f32, bf16 = jnp.float32, jnp.bfloat16

WQ, WK, WV, WS, WM, WG, WU, WD = range(8)


def rms(matrix):
    return matrix * lax.rsqrt(jnp.mean(matrix * matrix, axis=-1, keepdims=True) + norm_epsilon)


def silu(value):
    return value / (1.0 + jnp.exp(-value))


def dot(left, right):
    return jnp.dot(left, right, preferred_element_type=f32)


def ds(start, size, multiple=None):
    return pl.ds(pl.multiple_of(start, multiple or size), size)


MIXER = (WQ, WK, WV, WS, WM)
WHOLE = (WQ, WK, WV, WS, WG, WU, WD)


def layer(G, F, T, *refs):
    tokens, gains, cosine, sine = refs[:4]
    shards = refs[4:12]
    out = refs[12]
    bufs = refs[13:21]
    act, queries, keys, values, acc, send1, recv1, recv2 = refs[21:29]
    (local_sem, z_send, z_recv, y_send, y_recv, e_send, e_recv, ag_x_send, ag_x_recv, ag_c_send,
     ag_c_recv, rs1_send, rs1_recv, rs2_send, rs2_recv, client_sem, ret_send, ret_recv) = refs[29:]

    X = T // CORES
    g, f, t = lax.axis_index("grp"), lax.axis_index("fs"), lax.axis_index("tp")
    x, c = t // CORES, t % CORES
    R, D = tokens.shape
    L = R * T
    TM = min(256, L)
    heads = queries.shape[2] // QK
    VD = values.shape[2] // heads
    FH = bufs[WG].shape[1]
    total, after = acc.at[0], acc.at[1]
    partner = (g, f, x * CORES + (1 - c))

    moved = F >= 4
    is_end = (f == 0) | (f == F - 1) if moved else f < 0
    is_host = (f == 1) | (f == F - 2) if moved else f < 0
    not_end = jnp.logical_not(is_end)
    outer = jnp.where(f == 1, 0, F - 1)
    host = jnp.where(f == 0, 1, F - 2)

    def x_peer(o):
        return lax.rem(x + o, X)

    neighbours = [(f > 0, (g, f - 1, t)), (f < F - 1, (g, f + 1, t))]
    neighbours += [(None, (lax.rem(g + o, G), f, t)) for o in range(1, G)]
    neighbours += [(None, (g, f, x_peer(o) * CORES + c)) for o in range(1, X)]
    neighbours += [(None, partner)]

    def when(condition, action):
        if condition is None:
            action()
        else:
            pl.when(condition)(action)

    def local_copy(w):
        r = shards[w].shape[0]
        return pltpu.make_async_copy(shards[w], bufs[w].at[ds(f * r, r)], local_sem.at[w])

    def half(w, s, part):
        r = shards[w].shape[0]
        return bufs[w].at[ds(s * r + part * (r // G), r // G)]

    def source(d, k):
        return (f - k if d == 0 else f + k)

    def valid(d, k):
        return (f >= k if d == 0 else f + k < F)

    def has_next(w, d):
        margin = 1 if moved and w in MIXER else 0
        return f < F - 1 - margin if d == 0 else f > margin

    def takes(w, k, d):
        return valid(d, k) & not_end if w in MIXER else valid(d, k)

    def gives(w, k, d):
        return has_next(w, d) if k == 0 else takes(w, k, d) & has_next(w, d)

    def outward(d):
        return is_host & (f == F - 2 if d == 0 else f == 1)

    def from_end(d):
        return is_host & (f == 1 if d == 0 else f == F - 2)

    def crosses(w, k, d):
        if w in WHOLE and k == 1:
            return takes(w, k, d) & jnp.logical_not(from_end(d))
        return takes(w, k, d)

    def z_copy(w, k, d):
        region = half(w, source(d, k), g)
        return pltpu.make_async_remote_copy(
            region, region, z_send.at[d, w, k], z_recv.at[d, w, k + 1],
            device_id=(g, f + 1 if d == 0 else f - 1, t), device_id_type=MESH)

    def z_wait(w, k, d):
        region = half(w, source(d, k), g)
        pltpu.make_async_remote_copy(
            region, region, z_send.at[d, w, k], z_recv.at[d, w, k],
            device_id=(g, f, t), device_id_type=MESH).wait_recv()

    def y_copy(w, k, d, o):
        region = half(w, source(d, k), g)
        return pltpu.make_async_remote_copy(
            region, region, y_send.at[d, w, k, o], y_recv.at[d, w, k, o],
            device_id=(lax.rem(g + o, G), f, t), device_id_type=MESH)

    def y_wait(w, k, d, o):
        region = half(w, source(d, k), lax.rem(g + G - o, G))
        pltpu.make_async_remote_copy(
            region, region, y_send.at[d, w, k, o], y_recv.at[d, w, k, o],
            device_id=(g, f, t), device_id_type=MESH).wait_recv()

    def end_copy(w, o, s, device):
        region = half(w, s, lax.rem(g + o, G))
        return pltpu.make_async_remote_copy(
            region, region, e_send.at[w, o], e_recv.at[w, o],
            device_id=(g, device, t), device_id_type=MESH)

    def give_own(w, early):
        for d in range(2):
            if w in MIXER:
                condition = has_next(w, d)
            elif early:
                condition = outward(d)
            else:
                condition = has_next(w, d) & jnp.logical_not(outward(d))
            pl.when(condition)(lambda d=d: z_copy(w, 0, d).start())
        if w in WHOLE and not early:
            @pl.when(is_end)
            def _():
                for o in range(1, G):
                    end_copy(w, o, f, host).start()

    def comm(w, k):
        if k == 0:
            if w in MIXER:
                local_copy(w).wait()
            give_own(w, False)
            return
        for d in range(2):
            @pl.when(takes(w, k, d))
            def _(d=d):
                z_wait(w, k, d)
                if k < F - 1:
                    pl.when(has_next(w, d))(lambda: z_copy(w, k, d).start())
            @pl.when(crosses(w, k, d))
            def _(d=d):
                for o in range(1, G):
                    y_copy(w, k, d, o).start()

    def arrived_from(w, k, d):
        @pl.when(crosses(w, k, d))
        def _():
            for o in range(1, G):
                y_wait(w, k, d, o)
        if w in WHOLE and k == 1:
            @pl.when(from_end(d))
            def _():
                for o in range(1, G):
                    end_copy(w, o, source(d, k), f).wait_recv()

    def arrived(w):
        for k in range(1, F):
            for d in range(2):
                arrived_from(w, k, d)

    def drain(w):
        for k in range(F):
            for d in range(2):
                if k < F - 1:
                    pl.when(gives(w, k, d))(lambda k=k, d=d: z_copy(w, k, d).wait_send())
                if k > 0:
                    @pl.when(crosses(w, k, d))
                    def _(k=k, d=d):
                        for o in range(1, G):
                            y_copy(w, k, d, o).wait_send()
        if w in WHOLE:
            @pl.when(is_end)
            def _():
                for o in range(1, G):
                    end_copy(w, o, f, host).wait_send()

    def rows_of(q, device):
        return act.at[q, ds(device * R, R)]

    def slot(stage):
        return 1 if stage == 1 else 0

    def ag_x(stage, o):
        region = rows_of(slot(stage), t)
        return pltpu.make_async_remote_copy(
            region, region, ag_x_send.at[stage, o], ag_x_recv.at[stage, o],
            device_id=(g, f, x_peer(o) * CORES + c), device_id_type=MESH)

    def ag_c(stage, o, core):
        region = rows_of(slot(stage), x_peer(X - o) * CORES + core)
        return pltpu.make_async_remote_copy(
            region, region, ag_c_send.at[stage, o], ag_c_recv.at[stage, o],
            device_id=partner, device_id_type=MESH)

    def gather_start(stage):
        for o in range(1, X):
            ag_x(stage, o).start()
        ag_c(stage, 0, c).start()

    def gather_forward(stage):
        for o in range(1, X):
            region = rows_of(slot(stage), x_peer(X - o) * CORES + c)
            pltpu.make_async_remote_copy(
                region, region, ag_x_send.at[stage, o], ag_x_recv.at[stage, o],
                device_id=(g, f, t), device_id_type=MESH).wait_recv()
            ag_c(stage, o, c).start()

    def gather_wait(stage):
        for o in range(X):
            ag_c(stage, o, 1 - c).wait_recv()

    def gather_drain(stage):
        for o in range(X):
            if o:
                ag_x(stage, o).wait_send()
            ag_c(stage, o, c).wait_send()

    def client_copy(device):
        return pltpu.make_async_remote_copy(
            rows_of(0, t), rows_of(1, t), client_sem.at[0], client_sem.at[1],
            device_id=(g, device, t), device_id_type=MESH)

    cols = send1.shape[-1]

    def rs1(stage, q, j):
        return pltpu.make_async_remote_copy(
            send1.at[q, j], recv1.at[q, j], rs1_send.at[stage, j], rs1_recv.at[stage, j],
            device_id=partner, device_id_type=MESH)

    def rs2(stage, q, j, o):
        return pltpu.make_async_remote_copy(
            send1.at[q, j, o], recv2.at[q, j, o], rs2_send.at[stage, j, o],
            rs2_recv.at[stage, j, o],
            device_id=(g, f, x_peer(o) * CORES + c), device_id_type=MESH)

    def give_back(j, device):
        return pltpu.make_async_remote_copy(
            send1.at[1, j, 0], recv2.at[0, j, 0], ret_send.at[j], ret_recv.at[j],
            device_id=(g, device, t), device_id_type=MESH)

    def partial_rows(w, width, q, j, device):
        r = shards[w].shape[0]
        return dot(values[q, ds(device * R, R), :width], bufs[w][ds(j * r, r), :])

    def sum_send(stage, q, w, width, j):
        def one(o, _):
            send1[q, j, o] = partial_rows(w, width, q, j, o * CORES + (1 - c)).astype(bf16)
            return 0
        lax.fori_loop(0, X, one, 0)
        rs1(stage, q, j).start()

    def sum_pass(stage, q, w, width, j):
        rs1(stage, q, j).wait()
        def pair(o):
            peer = x_peer(o)
            return (partial_rows(w, width, q, j, peer * CORES + c)
                    + recv1[q, j, peer].astype(f32))
        for o in range(1, X):
            send1[q, j, o] = pair(o).astype(bf16)
            rs2(stage, q, j, o).start()
        acc[q, :, ds(j * cols, cols)] = pair(0)

    def sum_finish(stage, q, j):
        block = acc[q, :, ds(j * cols, cols)]
        for o in range(1, X):
            rs2(stage, q, j, o).wait_recv()
            block += recv2[q, j, o].astype(f32)
        return block

    def sum_drain(stage, q):
        def one(j, _):
            for o in range(1, X):
                rs2(stage, q, j, o).wait_send()
            return 0
        lax.fori_loop(0, F, one, 0)

    RT = min(32, R)

    def norm_in():
        def one(i, _):
            rows = ds(i * RT, RT)
            act[0, ds(t * R + i * RT, RT)] = (
                rms(tokens[rows].astype(f32)) * gains[0:1]).astype(bf16)
            return 0
        lax.fori_loop(0, R // RT, one, 0)

    def norm_mid():
        def one(i, _):
            rows = ds(i * RT, RT)
            mid = tokens[rows].astype(f32) + rms(total[rows]) * gains[1:2]
            after[rows] = mid
            act[0, ds(t * R + i * RT, RT)] = (rms(mid) * gains[2:3]).astype(bf16)
            return 0
        lax.fori_loop(0, R // RT, one, 0)

    def norm_out():
        def one(i, _):
            rows = ds(i * RT, RT)
            out[rows] = (after[rows] + rms(total[rows]) * gains[3:4]).astype(bf16)
            return 0
        lax.fori_loop(0, R // RT, one, 0)

    def tiles(width, tile, body):
        across = width // tile

        def one(i, _):
            body(ds((i // across) * TM, TM), ds((i % across) * tile, tile))
            return 0
        lax.fori_loop(0, (L // TM) * across, one, 0)

    def rotary(q, w, into, scale):
        def body(rows, cols):
            head = dot(act[q, rows], bufs[w][:, cols])
            lower, upper = head[:, :QK // 2], head[:, QK // 2:]
            cos, sin = cosine[rows], sine[rows]
            rotated = jnp.concatenate(
                [lower * cos - upper * sin, lower * sin + upper * cos], axis=-1)
            into[q, rows, cols] = (rotated * scale).astype(bf16)
        tiles(heads * QK, QK, body)

    def project_values(q):
        def body(rows, cols):
            values[q, rows, cols] = dot(act[q, rows], bufs[WV][:, cols]).astype(bf16)
        tiles(heads * VD, VD, body)

    def retain(q, h):
        head_index = (t * heads + h).astype(f32)
        fraction = jnp.full((1, 1), 1.0, f32) * (head_index / (heads * T - 1.0))
        log_decay = -(4.0 / BLOCK) * jnp.exp(fraction * math.log(BLOCK / (32.0 * L)))
        qk_cols = ds(h * QK, QK)
        v_cols = ds(h * VD, VD)
        for i in reversed(range(L // TM)):
            rows, seen = pl.ds(i * TM, TM), (i + 1) * TM
            scores = lax.dot_general(
                queries[q, rows, qk_cols], keys[q, :seen, qk_cols], (((1,), (1,)), ((), ())),
                preferred_element_type=f32)
            distance = (lax.broadcasted_iota(jnp.int32, (TM, seen), 0) + i * TM
                        - lax.broadcasted_iota(jnp.int32, (TM, seen), 1)).astype(f32)
            weights = jnp.where(
                distance >= 0, jnp.exp(log_decay * jnp.maximum(distance, 0.0)), 0.0)
            retained = dot((scores * weights).astype(bf16), values[q, :seen, v_cols])
            centred = retained - jnp.mean(retained, axis=-1, keepdims=True)
            normalized = centred * lax.rsqrt(
                jnp.mean(centred * centred, axis=-1, keepdims=True) + group_epsilon)
            swish = dot(act[q, rows], bufs[WS][:, v_cols])
            values[q, rows, v_cols] = (silu(swish) * normalized).astype(bf16)

    def retain_all(q):
        lax.fori_loop(0, heads, lambda h, _: (retain(q, h), 0)[1], 0)

    def hidden_units():
        def body(rows, cols):
            up = dot(act[0, rows], bufs[WU][:, cols])
            gate = dot(act[0, rows], bufs[WG][:, cols])
            values[0, rows, cols] = (silu(gate) * up).astype(bf16)
        tiles(FH, math.gcd(FH, 256), body)

    for w in range(8):
        local_copy(w).start()
    barrier = pltpu.get_barrier_semaphore()
    for condition, device in neighbours:
        when(condition, lambda device=device: pl.semaphore_signal(
            barrier, inc=1, device_id=device, device_id_type=MESH))
    fixed = (G - 1) + (X - 1) + 1
    pl.semaphore_wait(
        barrier, fixed + (f > 0).astype(jnp.int32) + (f < F - 1).astype(jnp.int32))

    comm(WQ, 0)
    norm_in()
    pl.when(is_end)(lambda: client_copy(host).start())
    pl.when(not_end)(lambda: gather_start(0))
    comm(WK, 0)
    for w in (WG, WU, WD):
        local_copy(w).wait()
        give_own(w, True)
    for k in range(1, F):
        comm(WQ, k)
    comm(WV, 0)
    comm(WK, 1)
    pl.when(not_end)(lambda: gather_forward(0))
    for k in range(2, F):
        comm(WK, k)
    comm(WS, 0)

    @pl.when(not_end)
    def _():
        gather_wait(0)
        arrived(WQ)
        rotary(0, WQ, queries, 1.0)
    comm(WV, 1)

    @pl.when(is_host)
    def _():
        client_copy(f).wait_recv()
        gather_start(1)

    @pl.when(not_end)
    def _():
        arrived(WK)
        rotary(0, WK, keys, QK ** -0.5)
    for k in range(2, F):
        comm(WV, k)
    comm(WM, 0)
    comm(WS, 1)

    @pl.when(not_end)
    def _():
        arrived(WV)
        project_values(0)
    pl.when(is_host)(lambda: gather_forward(1))
    comm(WG, 0)
    for k in range(2, F):
        comm(WS, k)

    @pl.when(is_host)
    def _():
        gather_wait(1)
        rotary(1, WQ, queries, 1.0)
        rotary(1, WK, keys, QK ** -0.5)
    comm(WM, 1)
    pl.when(is_host)(lambda: project_values(1))
    pl.when(not_end)(lambda: arrived(WS))
    if F > 2:
        comm(WM, 2)
    pl.when(is_host)(lambda: retain_all(1))
    for k in range(3, F):
        comm(WM, k)
    comm(WU, 0)
    pl.when(not_end)(lambda: retain_all(0))
    comm(WG, 1)
    pl.when(not_end)(lambda: gather_drain(0))

    slots = jnp.where(is_end, 0, jnp.where(is_host, 2, 1))

    def mixer(d, k):
        j = source(d, k)

        def one(n, _):
            q = slots - 1 - n
            sum_send(q, q, WM, heads * VD, j)
            return 0

        def two(n, _):
            q = slots - 1 - n
            sum_pass(q, q, WM, heads * VD, j)
            return 0
        lax.fori_loop(0, slots, one, 0)
        lax.fori_loop(0, slots, two, 0)

    mixer(0, 0)
    for k in range(1, F):
        for d in range(2):
            @pl.when(takes(WM, k, d))
            def _(k=k, d=d):
                arrived_from(WM, k, d)
                mixer(d, k)
    for k in range(2, F):
        comm(WG, k)
    comm(WD, 0)

    @pl.when(is_host)
    def _():
        def one(j, _):
            send1[1, j, 0] = sum_finish(1, 1, j).astype(bf16)
            give_back(j, outer).start()
            return 0
        lax.fori_loop(0, F, one, 0)

    @pl.when(not_end)
    def _():
        def one(j, _):
            acc[0, :, ds(j * cols, cols)] = sum_finish(0, 0, j)
            return 0
        lax.fori_loop(0, F, one, 0)
        sum_drain(0, 0)
    comm(WU, 1)

    @pl.when(is_end)
    def _():
        client_copy(host).wait_send()

        def one(j, _):
            give_back(j, f).wait_recv()
            acc[0, :, ds(j * cols, cols)] = recv2[0, j, 0].astype(f32)
            return 0
        lax.fori_loop(0, F, one, 0)
    norm_mid()
    gather_start(2)
    for k in range(2, F):
        comm(WU, k)
    comm(WD, 1)
    gather_forward(2)
    gather_wait(2)
    arrived(WG)
    arrived(WU)
    hidden_units()

    def down(j):
        sum_send(2, 0, WD, FH, j)
        sum_pass(2, 0, WD, FH, j)
    down(f)
    for k in range(1, F):
        if k > 1:
            comm(WD, k)
        for d in range(2):
            @pl.when(takes(WD, k, d))
            def _(k=k, d=d):
                arrived_from(WD, k, d)
                down(source(d, k))

    def finish(j, _):
        acc[0, :, ds(j * cols, cols)] = sum_finish(2, 0, j)
        return 0
    lax.fori_loop(0, F, finish, 0)
    norm_out()
    gather_drain(2)
    sum_drain(2, 0)

    @pl.when(is_host)
    def _():
        gather_drain(1)
        sum_drain(1, 1)

        def one(j, _):
            give_back(j, outer).wait_send()
            return 0
        lax.fori_loop(0, F, one, 0)
    for w in range(8):
        drain(w)


def per_device(tokens, norm_gains, *weights):
    G, F, T = lax.axis_size("grp"), lax.axis_size("fs"), lax.axis_size("tp")
    X = T // CORES
    R, D = tokens.shape
    L = R * T
    query, _, value, _, mixer, gate, _, down = weights
    qk_width, v_width, hidden = query.shape[1], value.shape[1], gate.shape[1]
    positions = jnp.arange(L, dtype=f32)
    frequency = 10000.0 ** (-jnp.linspace(0.0, 1.0, QK // 2, dtype=f32))
    angles = positions[:, None] * frequency[None, :]
    vmem = pl.BlockSpec(memory_space=pltpu.VMEM)
    anywhere = pl.BlockSpec(memory_space=pl.ANY)
    DMA = pltpu.SemaphoreType.DMA
    cols = mixer.shape[1]
    scratch = [pltpu.VMEM((w.shape[0] * F, w.shape[1]), bf16) for w in weights]
    scratch += [
        pltpu.VMEM((2, L, D), bf16),
        pltpu.VMEM((2, L, qk_width), bf16),
        pltpu.VMEM((2, L, qk_width), bf16),
        pltpu.VMEM((2, L, max(v_width, hidden)), bf16),
        pltpu.VMEM((2, R, D), f32),
        pltpu.VMEM((2, F, X, R, cols), bf16),
        pltpu.VMEM((2, F, X, R, cols), bf16),
        pltpu.VMEM((2, F, X, R, cols), bf16),
        DMA((8,)),
        DMA((2, 8, F)), DMA((2, 8, F)), DMA((2, 8, F, G)), DMA((2, 8, F, G)),
        DMA((8, G)), DMA((8, G)),
        DMA((3, X)), DMA((3, X)), DMA((3, X)), DMA((3, X)),
        DMA((3, F)), DMA((3, F)), DMA((3, F, X)), DMA((3, F, X)),
        DMA((2,)), DMA((F,)), DMA((F,)),
    ]
    return pl.pallas_call(
        functools.partial(layer, G, F, T),
        out_shape=jax.ShapeDtypeStruct((R, D), bf16),
        in_specs=[vmem] * 4 + [anywhere] * 8,
        out_specs=vmem,
        scratch_shapes=scratch,
        compiler_params=pltpu.CompilerParams(
            collective_id=0, has_side_effects=True, vmem_limit_bytes=67043328),
    )(tokens, norm_gains, jnp.cos(angles), jnp.sin(angles), *weights)


def solution(mesh):
    placed = (
        P(("grp", "fs", "tp"), None),
        P(),
        P("fs", "tp"),
        P("fs", "tp"),
        P("fs", "tp"),
        P("fs", "tp"),
        P("tp", "fs"),
        P("fs", "tp"),
        P("fs", "tp"),
        P("tp", "fs"),
    )
    return jax.shard_map(
        per_device,
        mesh=mesh,
        in_specs=placed,
        out_specs=P(("grp", "fs", "tp"), None),
        check_vma=False,
    )
```

time: 286 us -> 295 us (1.031); the launches traced: 282 us -> 295 us
  Pallas kernels: 276 us -> 290 us
    pallas_call x1, Pallas kernels: 276 us -> 290 us  [per_device(): pl.pallas_call(functools.partial(layer, G, F, T), out_shape=jax.ShapeDtyp...]
where the time goes in v1:
time: 295 us
  Pallas kernels  290 us (98%)
    pallas_call x1, Pallas kernels, per_device(): pl.pallas_call(functools.partial(layer, G, F, T), out_shape=jax.ShapeDtyp...  290 us

profile of v1, /device:TPU:24, one launch (start us, length us, event | category | flops | bytes accessed | tf_op | source)
XLA Modules:
  0.0 294.7 jit_solution(3433354075256038108)
XLA Ops:
  0.0 0.1 fusion.2
  0.1 2.8 fusion
  2.9 289.5 %shard_map.100 = bf16[256,2048]{1,0:T(8,128)(2,1)} custom-call(bf16[256,2048]{1,0:T(8,128)(2,1)} %refs_0_.1, f32[4,2048]{1,0:T(4,128)} %refs_1_.1, f32[1024,128]{1,0:T(8,128)} %get-tuple-element.6.refs_2_, f32[1024,128]{1,0:T(8,128)} %get-tuple-element.5.refs_3_, bf16[512,512]{1,0:T(8,128)(2,1)} %refs_4_.1, bf16[512,512]{1,0:T(8,128)(2,1)} %refs_5_.1, ...), custom_call_target="tpu_custom_call" | custom-call | tf_op jit(solution)/shard_map/pallas_call | solution.py:601
  292.4 2.3 copy.12
  (1 shorter events, 0.0 us)

commit v2 on v1

--- a/solution.py
+++ b/solution.py
@@ -91,15 +91,22 @@
         r = shards[w].shape[0]
         return bufs[w].at[ds(s * r + part * (r // G), r // G)]
 
+    left = f * 2 < F
+    ways = (jnp.where(left, 1, 0), jnp.where(left, 0, 1))
+    steps = (2 * ways[0] - 1, 2 * ways[1] - 1)
+
     def source(d, k):
-        return (f - k if d == 0 else f + k)
+        return f + steps[d] * k
+
+    def target(d):
+        return f - steps[d]
 
     def valid(d, k):
-        return (f >= k if d == 0 else f + k < F)
+        return (source(d, k) >= 0) & (source(d, k) < F)
 
     def has_next(w, d):
         margin = 1 if moved and w in MIXER else 0
-        return f < F - 1 - margin if d == 0 else f > margin
+        return (target(d) >= margin) & (target(d) <= F - 1 - margin)
 
     def takes(w, k, d):
         return valid(d, k) & not_end if w in MIXER else valid(d, k)
@@ -107,39 +114,37 @@
     def gives(w, k, d):
         return has_next(w, d) if k == 0 else takes(w, k, d) & has_next(w, d)
 
-    def outward(d):
-        return is_host & (f == F - 2 if d == 0 else f == 1)
-
-    def from_end(d):
-        return is_host & (f == 1 if d == 0 else f == F - 2)
+    def from_end(w, k, d):
+        return is_host if w in WHOLE and k == 1 and d == 1 else None
 
     def crosses(w, k, d):
-        if w in WHOLE and k == 1:
-            return takes(w, k, d) & jnp.logical_not(from_end(d))
-        return takes(w, k, d)
+        special = from_end(w, k, d)
+        if special is None:
+            return takes(w, k, d)
+        return takes(w, k, d) & jnp.logical_not(special)
 
     def z_copy(w, k, d):
         region = half(w, source(d, k), g)
         return pltpu.make_async_remote_copy(
-            region, region, z_send.at[d, w, k], z_recv.at[d, w, k + 1],
-            device_id=(g, f + 1 if d == 0 else f - 1, t), device_id_type=MESH)
+            region, region, z_send.at[ways[d], w, k], z_recv.at[ways[d], w, k + 1],
+            device_id=(g, target(d), t), device_id_type=MESH)
 
     def z_wait(w, k, d):
         region = half(w, source(d, k), g)
         pltpu.make_async_remote_copy(
-            region, region, z_send.at[d, w, k], z_recv.at[d, w, k],
+            region, region, z_send.at[ways[d], w, k], z_recv.at[ways[d], w, k],
             device_id=(g, f, t), device_id_type=MESH).wait_recv()
 
     def y_copy(w, k, d, o):
         region = half(w, source(d, k), g)
         return pltpu.make_async_remote_copy(
-            region, region, y_send.at[d, w, k, o], y_recv.at[d, w, k, o],
+            region, region, y_send.at[ways[d], w, k, o], y_recv.at[ways[d], w, k, o],
             device_id=(lax.rem(g + o, G), f, t), device_id_type=MESH)
 
     def y_wait(w, k, d, o):
         region = half(w, source(d, k), lax.rem(g + G - o, G))
         pltpu.make_async_remote_copy(
-            region, region, y_send.at[d, w, k, o], y_recv.at[d, w, k, o],
+            region, region, y_send.at[ways[d], w, k, o], y_recv.at[ways[d], w, k, o],
             device_id=(g, f, t), device_id_type=MESH).wait_recv()
 
     def end_copy(w, o, s, device):
@@ -153,52 +158,76 @@
             if w in MIXER:
                 condition = has_next(w, d)
             elif early:
-                condition = outward(d)
+                condition = is_host if d == 0 else None
             else:
-                condition = has_next(w, d) & jnp.logical_not(outward(d))
-            pl.when(condition)(lambda d=d: z_copy(w, 0, d).start())
-        if w in WHOLE and not early:
-            @pl.when(is_end)
-            def _():
-                for o in range(1, G):
-                    end_copy(w, o, f, host).start()
-
-    def comm(w, k):
-        if k == 0:
-            if w in MIXER:
-                local_copy(w).wait()
-            give_own(w, False)
-            return
-        for d in range(2):
-            @pl.when(takes(w, k, d))
-            def _(d=d):
-                z_wait(w, k, d)
-                if k < F - 1:
-                    pl.when(has_next(w, d))(lambda: z_copy(w, k, d).start())
-            @pl.when(crosses(w, k, d))
-            def _(d=d):
-                for o in range(1, G):
-                    y_copy(w, k, d, o).start()
-
-    def arrived_from(w, k, d):
-        @pl.when(crosses(w, k, d))
+                condition = has_next(w, d)
+                if d == 0:
+                    condition &= jnp.logical_not(is_host)
+            if condition is not None:
+                pl.when(condition)(lambda d=d: z_copy(w, 0, d).start())
+
+    def give_rest(w):
+        @pl.when(is_end)
+        def _():
+            for o in range(1, G):
+                end_copy(w, o, f, host).start()
+
+    def comm0(w):
+        if w in MIXER:
+            local_copy(w).wait()
+        give_own(w, False)
+
+    def pass_on(w, k, d, who=None):
+        if k < F - 1:
+            condition = gives(w, k, d)
+            pl.when(condition if who is None else condition & who)(
+                lambda: z_copy(w, k, d).start())
+
+    def along_z(w, k, d, who=None, onward=True):
+        pl.when(takes(w, k, d) if who is None else takes(w, k, d) & who)(
+            lambda: z_wait(w, k, d))
+        if onward:
+            pass_on(w, k, d, who)
+
+    def along_y(w, k, d, who=None):
+        @pl.when(crosses(w, k, d) if who is None else crosses(w, k, d) & who)
+        def _():
+            for o in range(1, G):
+                y_copy(w, k, d, o).start()
+
+    def comm(w, k, d, who=None):
+        along_z(w, k, d, who)
+        along_y(w, k, d, who)
+
+    reach = (range(1, F), range(1, (F - 1) // 2 + 1))
+
+    def rest(w, d, who=None):
+        for k in reach[d][1:]:
+            comm(w, k, d, who)
+
+    def arrived_from(w, k, d, who=None):
+        def narrow(condition):
+            return condition if who is None else condition & who
+
+        @pl.when(narrow(crosses(w, k, d)))
         def _():
             for o in range(1, G):
                 y_wait(w, k, d, o)
-        if w in WHOLE and k == 1:
-            @pl.when(from_end(d))
+        special = from_end(w, k, d)
+        if special is not None:
+            @pl.when(narrow(special))
             def _():
                 for o in range(1, G):
                     end_copy(w, o, source(d, k), f).wait_recv()
 
     def arrived(w):
-        for k in range(1, F):
-            for d in range(2):
+        for d in range(2):
+            for k in reach[d]:
                 arrived_from(w, k, d)
 
     def drain(w):
-        for k in range(F):
-            for d in range(2):
+        for d in range(2):
+            for k in (0, *reach[d]):
                 if k < F - 1:
                     pl.when(gives(w, k, d))(lambda k=k, d=d: z_copy(w, k, d).wait_send())
                 if k > 0:
@@ -235,13 +264,16 @@
             ag_x(stage, o).start()
         ag_c(stage, 0, c).start()
 
+    def gather_forward_one(stage, o):
+        region = rows_of(slot(stage), x_peer(X - o) * CORES + c)
+        pltpu.make_async_remote_copy(
+            region, region, ag_x_send.at[stage, o], ag_x_recv.at[stage, o],
+            device_id=(g, f, t), device_id_type=MESH).wait_recv()
+        ag_c(stage, o, c).start()
+
     def gather_forward(stage):
         for o in range(1, X):
-            region = rows_of(slot(stage), x_peer(X - o) * CORES + c)
-            pltpu.make_async_remote_copy(
-                region, region, ag_x_send.at[stage, o], ag_x_recv.at[stage, o],
-                device_id=(g, f, t), device_id_type=MESH).wait_recv()
-            ag_c(stage, o, c).start()
+            gather_forward_one(stage, o)
 
     def gather_wait(stage):
         for o in range(X):
@@ -380,18 +412,65 @@
             centred = retained - jnp.mean(retained, axis=-1, keepdims=True)
             normalized = centred * lax.rsqrt(
                 jnp.mean(centred * centred, axis=-1, keepdims=True) + group_epsilon)
-            swish = dot(act[q, rows], bufs[WS][:, v_cols])
-            values[q, rows, v_cols] = (silu(swish) * normalized).astype(bf16)
+            values[q, rows, v_cols] = normalized.astype(bf16)
 
     def retain_all(q):
         lax.fori_loop(0, heads, lambda h, _: (retain(q, h), 0)[1], 0)
 
-    def hidden_units():
+    def project_swish(q):
         def body(rows, cols):
+            swish = dot(act[q, rows], bufs[WS][:, cols])
+            values[q, rows, cols] = (
+                silu(swish) * values[q, rows, cols].astype(f32)).astype(bf16)
+        tiles(heads * VD, VD, body)
+
+    def hidden_units(device):
+        tile = math.gcd(FH, 256)
+
+        def one(i, _):
+            rows, cols = ds(device * R, R), ds(i * tile, tile)
             up = dot(act[0, rows], bufs[WU][:, cols])
             gate = dot(act[0, rows], bufs[WG][:, cols])
             values[0, rows, cols] = (silu(gate) * up).astype(bf16)
-        tiles(FH, math.gcd(FH, 256), body)
+            return 0
+        lax.fori_loop(0, FH // tile, one, 0)
+
+    def sums(stage, q, w, width, items, who=None, first=None):
+        def condition(k, d):
+            if k == 0:
+                return who
+            return takes(w, k, d) if who is None else takes(w, k, d) & who
+
+        for n in range(len(items) + 1):
+            if n < len(items):
+                k, d = items[n]
+                if k:
+                    arrived_from(w, k, d, first)
+                when(condition(k, d), lambda k=k, d=d: sum_send(stage, q, w, width, source(d, k)))
+            if n > 0:
+                k, d = items[n - 1]
+                when(condition(k, d), lambda k=k, d=d: sum_pass(stage, q, w, width, source(d, k)))
+
+    def finish_client(j):
+        send1[1, j, 0] = sum_finish(1, 1, j).astype(bf16)
+        give_back(j, outer).start()
+
+    def finish_own(stage):
+        def one(j, _):
+            acc[0, :, ds(j * cols, cols)] = sum_finish(stage, 0, j)
+            return 0
+        lax.fori_loop(0, F, one, 0)
+
+    def take_back():
+        def one(j, _):
+            give_back(j, f).wait_recv()
+            acc[0, :, ds(j * cols, cols)] = recv2[0, j, 0].astype(f32)
+            return 0
+        lax.fori_loop(0, F, one, 0)
+
+    far = [(k, d) for k in range(2, F) for d in range(2) if k in reach[d]]
+    near = [(0, 0), (1, 0), (1, 1)]
+    guest = not_end & jnp.logical_not(is_host)
 
     for w in range(8):
         local_copy(w).start()
@@ -403,153 +482,159 @@
     pl.semaphore_wait(
         barrier, fixed + (f > 0).astype(jnp.int32) + (f < F - 1).astype(jnp.int32))
 
-    comm(WQ, 0)
+    comm0(WQ)
+    give_rest(WQ)
     norm_in()
     pl.when(is_end)(lambda: client_copy(host).start())
     pl.when(not_end)(lambda: gather_start(0))
-    comm(WK, 0)
+    comm0(WK)
     for w in (WG, WU, WD):
         local_copy(w).wait()
         give_own(w, True)
-    for k in range(1, F):
-        comm(WQ, k)
-    comm(WV, 0)
-    comm(WK, 1)
-    pl.when(not_end)(lambda: gather_forward(0))
-    for k in range(2, F):
-        comm(WK, k)
-    comm(WS, 0)
+    comm(WQ, 1, 0)
+    comm(WQ, 1, 1)
+    rest(WQ, 0)
+    rest(WQ, 1)
+    comm0(WV)
+    comm(WK, 1, 0)
 
     @pl.when(not_end)
     def _():
+        gather_forward(0)
         gather_wait(0)
         arrived(WQ)
         rotary(0, WQ, queries, 1.0)
-    comm(WV, 1)
+    comm(WV, 1, 0)
+    give_rest(WK)
+    comm0(WS)
+    give_rest(WV)
+    give_rest(WS)
 
     @pl.when(is_host)
     def _():
         client_copy(f).wait_recv()
         gather_start(1)
+    comm(WK, 1, 1)
+    rest(WK, 0)
+    rest(WK, 1)
+    comm(WS, 1, 0)
+    comm(WV, 1, 1)
+    comm0(WM)
+
+    @pl.when(is_end)
+    def _():
+        for w in (WG, WU, WD):
+            give_own(w, False)
+        for w in (WG, WU, WD):
+            give_rest(w)
 
     @pl.when(not_end)
     def _():
         arrived(WK)
         rotary(0, WK, keys, QK ** -0.5)
-    for k in range(2, F):
-        comm(WV, k)
-    comm(WM, 0)
-    comm(WS, 1)
-
-    @pl.when(not_end)
-    def _():
-        arrived(WV)
-        project_values(0)
-    pl.when(is_host)(lambda: gather_forward(1))
-    comm(WG, 0)
-    for k in range(2, F):
-        comm(WS, k)
 
     @pl.when(is_host)
     def _():
+        gather_forward(1)
         gather_wait(1)
         rotary(1, WQ, queries, 1.0)
-        rotary(1, WK, keys, QK ** -0.5)
-    comm(WM, 1)
+    rest(WV, 0)
+    rest(WV, 1)
+    comm(WS, 1, 1)
+    pl.when(is_host)(lambda: rotary(1, WK, keys, QK ** -0.5))
+    pl.when(not_end)(lambda: arrived(WV))
     pl.when(is_host)(lambda: project_values(1))
+    rest(WS, 0)
+    rest(WS, 1)
+
+    @pl.when(not_end)
+    def _():
+        give_own(WG, False)
+        give_own(WU, False)
+        give_own(WD, False)
+    comm(WM, 1, 0)
+    pl.when(is_host)(lambda: retain_all(1))
+    pl.when(not_end)(lambda: project_values(0))
+    along_z(WG, 1, 0)
+    along_y(WG, 1, 0, is_end)
+    pl.when(not_end)(lambda: retain_all(0))
     pl.when(not_end)(lambda: arrived(WS))
-    if F > 2:
-        comm(WM, 2)
-    pl.when(is_host)(lambda: retain_all(1))
+    pl.when(is_host)(lambda: project_swish(1))
+    comm(WM, 1, 1)
+    along_z(WU, 1, 0)
+    along_y(WU, 1, 0, is_end)
+    sums(1, 1, WM, heads * VD, near[:2], is_host, is_host)
+    comm(WG, 1, 1)
+    along_z(WD, 1, 0)
+    along_y(WD, 1, 0, is_end)
+    pl.when(not_end)(lambda: project_swish(0))
+    along_y(WG, 1, 0, not_end)
+    pl.when(not_end)(lambda: gather_drain(0))
+
+    @pl.when(is_host)
+    def _():
+        finish_client(f)
+        finish_client(source(0, 1))
+    sums(0, 0, WM, heads * VD, near[:1], not_end, guest)
+    comm(WU, 1, 1)
+    rest(WM, 0)
+    rest(WM, 1)
+    sums(1, 1, WM, heads * VD, near[2:], is_host, is_host)
+    along_y(WU, 1, 0, not_end)
+    sums(0, 0, WM, heads * VD, near[1:2], not_end, guest)
+    rest(WG, 0, not_end)
+    rest(WG, 1)
+    comm(WD, 1, 1)
+    sums(1, 1, WM, heads * VD, far, is_host, is_host)
+    sums(0, 0, WM, heads * VD, near[2:] + far, not_end, guest)
+    pl.when(is_host)(lambda: finish_client(source(1, 1)))
+    for k in range(2, F):
+        along_z(WU, k, 0, not_end, False)
+        along_y(WU, k, 0, not_end)
+    rest(WU, 1)
+    along_y(WD, 1, 0, not_end)
+    for k, d in far:
+        pl.when(takes(WM, k, d) & is_host)(lambda k=k, d=d: finish_client(source(d, k)))
+    for k in range(2, F):
+        pass_on(WU, k, 0, not_end)
+    rest(WD, 0, not_end)
+    rest(WD, 1)
+    for w in (WG, WU, WD):
+        comm(w, 2, 0, is_end)
     for k in range(3, F):
-        comm(WM, k)
-    comm(WU, 0)
-    pl.when(not_end)(lambda: retain_all(0))
-    comm(WG, 1)
-    pl.when(not_end)(lambda: gather_drain(0))
-
-    slots = jnp.where(is_end, 0, jnp.where(is_host, 2, 1))
-
-    def mixer(d, k):
-        j = source(d, k)
-
-        def one(n, _):
-            q = slots - 1 - n
-            sum_send(q, q, WM, heads * VD, j)
-            return 0
-
-        def two(n, _):
-            q = slots - 1 - n
-            sum_pass(q, q, WM, heads * VD, j)
-            return 0
-        lax.fori_loop(0, slots, one, 0)
-        lax.fori_loop(0, slots, two, 0)
-
-    mixer(0, 0)
-    for k in range(1, F):
-        for d in range(2):
-            @pl.when(takes(WM, k, d))
-            def _(k=k, d=d):
-                arrived_from(WM, k, d)
-                mixer(d, k)
-    for k in range(2, F):
-        comm(WG, k)
-    comm(WD, 0)
-
-    @pl.when(is_host)
-    def _():
-        def one(j, _):
-            send1[1, j, 0] = sum_finish(1, 1, j).astype(bf16)
-            give_back(j, outer).start()
-            return 0
-        lax.fori_loop(0, F, one, 0)
+        comm(WG, k, 0, is_end)
+
+    @pl.when(is_end)
+    def _():
+        client_copy(host).wait_send()
+        take_back()
+        norm_mid()
+        gather_start(2)
 
     @pl.when(not_end)
     def _():
-        def one(j, _):
-            acc[0, :, ds(j * cols, cols)] = sum_finish(0, 0, j)
-            return 0
-        lax.fori_loop(0, F, one, 0)
+        finish_own(0)
         sum_drain(0, 0)
-    comm(WU, 1)
-
-    @pl.when(is_end)
-    def _():
-        client_copy(host).wait_send()
-
-        def one(j, _):
-            give_back(j, f).wait_recv()
-            acc[0, :, ds(j * cols, cols)] = recv2[0, j, 0].astype(f32)
-            return 0
-        lax.fori_loop(0, F, one, 0)
-    norm_mid()
-    gather_start(2)
-    for k in range(2, F):
-        comm(WU, k)
-    comm(WD, 1)
-    gather_forward(2)
-    gather_wait(2)
+        norm_mid()
+        gather_start(2)
+    for k in range(3, F):
+        comm(WU, k, 0, is_end)
+        comm(WD, k, 0, is_end)
     arrived(WG)
     arrived(WU)
-    hidden_units()
-
-    def down(j):
-        sum_send(2, 0, WD, FH, j)
-        sum_pass(2, 0, WD, FH, j)
-    down(f)
-    for k in range(1, F):
-        if k > 1:
-            comm(WD, k)
-        for d in range(2):
-            @pl.when(takes(WD, k, d))
-            def _(k=k, d=d):
-                arrived_from(WD, k, d)
-                down(source(d, k))
-
-    def finish(j, _):
-        acc[0, :, ds(j * cols, cols)] = sum_finish(2, 0, j)
-        return 0
-    lax.fori_loop(0, F, finish, 0)
+    ag_c(2, 0, 1 - c).wait_recv()
+    hidden_units(t)
+    hidden_units(x * CORES + 1 - c)
+    for o in range(1, X):
+        gather_forward_one(2, o)
+        hidden_units(x_peer(X - o) * CORES + c)
+    for o in range(1, X):
+        ag_c(2, o, 1 - c).wait_recv()
+        hidden_units(x_peer(X - o) * CORES + 1 - c)
+    sums(2, 0, WD, FH, near)
+    for k, d in far:
+        sums(2, 0, WD, FH, [(k, d)])
+    finish_own(2)
     norm_out()
     gather_drain(2)
     sum_drain(2, 0)

time: 295 us -> 242 us (0.82); the launches traced: 295 us -> 238 us
  Pallas kernels: 290 us -> 233 us
    pallas_call x1, Pallas kernels: 290 us -> 233 us  [per_device(): pl.pallas_call(functools.partial(layer, G, F, T), out_shape=jax.ShapeDtyp...]
where the time goes in v2:
time: 242 us; the launch traced here: 238 us
  Pallas kernels  233 us (96%)
  other arithmetic  2.9 us (1%)
    pallas_call x1, Pallas kernels, per_device(): pl.pallas_call(functools.partial(layer, G, F, T), out_shape=jax.ShapeDtyp...  233 us

profile of v2, /device:TPU:24, one launch (start us, length us, event | category | flops | bytes accessed | tf_op | source)
XLA Modules:
  0.0 238.5 jit_solution(16496374036879115380)
XLA Ops:
  0.0 0.1 fusion.2
  0.1 2.8 %fusion = (f32[1024,128]{1,0:T(8,128)}, f32[1024,128]{1,0:T(8,128)}) fusion(f32[128]{0:T(128)S(1)} %fusion.2), kind=kLoop, calls=%fused_computation.1 | loop fusion | flops 131072 | bytes 1049088 | tf_op jit(solution)/shard_map/sin | solution.py:694
  2.9 233.3 %shard_map.100 = bf16[256,2048]{1,0:T(8,128)(2,1)} custom-call(bf16[256,2048]{1,0:T(8,128)(2,1)} %refs_0_.1, f32[4,2048]{1,0:T(4,128)} %refs_1_.1, f32[1024,128]{1,0:T(8,128)} %get-tuple-element.6.refs_2_, f32[1024,128]{1,0:T(8,128)} %get-tuple-element.5.refs_3_, bf16[512,512]{1,0:T(8,128)(2,1)} %refs_4_.1, bf16[512,512]{1,0:T(8,128)(2,1)} %refs_5_.1, ...), custom_call_target="tpu_custom_call" | custom-call | tf_op jit(solution)/shard_map/pallas_call | solution.py:686
  236.2 2.3 copy.12
  (1 shorter events, 0.0 us)

commit v3 on v2

--- a/solution.py
+++ b/solution.py
@@ -3,6 +3,7 @@
 
 import jax
 import jax.numpy as jnp
+import numpy as np
 from jax import lax
 from jax.experimental import pallas as pl
 from jax.experimental.pallas import tpu as pltpu
@@ -42,13 +43,14 @@
 
 
 def layer(G, F, T, *refs):
-    tokens, gains, cosine, sine = refs[:4]
+    tokens, gains, coarse, fine = refs[:4]
     shards = refs[4:12]
     out = refs[12]
     bufs = refs[13:21]
     act, queries, keys, values, acc, send1, recv1, recv2 = refs[21:29]
+    cosine, sine, rows_out = refs[29:32]
     (local_sem, z_send, z_recv, y_send, y_recv, e_send, e_recv, ag_x_send, ag_x_recv, ag_c_send,
-     ag_c_recv, rs1_send, rs1_recv, rs2_send, rs2_recv, client_sem, ret_send, ret_recv) = refs[29:]
+     ag_c_recv, rs1_send, rs1_recv, rs2_send, rs2_recv, client_sem, ret_send, ret_recv, out_sem) = refs[32:]
 
     X = T // CORES
     g, f, t = lax.axis_index("grp"), lax.axis_index("fs"), lax.axis_index("tp")
@@ -123,34 +125,40 @@
             return takes(w, k, d)
         return takes(w, k, d) & jnp.logical_not(special)
 
+    def z_place(d, k):
+        return k if d == 0 else F - 1 + k
+
+    def y_place(d, k):
+        return k - 1 if d == 0 else F - 2 + k
+
     def z_copy(w, k, d):
         region = half(w, source(d, k), g)
         return pltpu.make_async_remote_copy(
-            region, region, z_send.at[ways[d], w, k], z_recv.at[ways[d], w, k + 1],
+            region, region, z_send.at[w, z_place(d, k)], z_recv.at[w, source(d, k)],
             device_id=(g, target(d), t), device_id_type=MESH)
 
     def z_wait(w, k, d):
         region = half(w, source(d, k), g)
         pltpu.make_async_remote_copy(
-            region, region, z_send.at[ways[d], w, k], z_recv.at[ways[d], w, k],
+            region, region, z_send.at[w, 0], z_recv.at[w, source(d, k)],
             device_id=(g, f, t), device_id_type=MESH).wait_recv()
 
     def y_copy(w, k, d, o):
         region = half(w, source(d, k), g)
         return pltpu.make_async_remote_copy(
-            region, region, y_send.at[ways[d], w, k, o], y_recv.at[ways[d], w, k, o],
+            region, region, y_send.at[w, y_place(d, k), o - 1], y_recv.at[w, y_place(d, k), o - 1],
             device_id=(lax.rem(g + o, G), f, t), device_id_type=MESH)
 
     def y_wait(w, k, d, o):
         region = half(w, source(d, k), lax.rem(g + G - o, G))
         pltpu.make_async_remote_copy(
-            region, region, y_send.at[ways[d], w, k, o], y_recv.at[ways[d], w, k, o],
+            region, region, y_send.at[w, y_place(d, k), o - 1], y_recv.at[w, y_place(d, k), o - 1],
             device_id=(g, f, t), device_id_type=MESH).wait_recv()
 
     def end_copy(w, o, s, device):
         region = half(w, s, lax.rem(g + o, G))
         return pltpu.make_async_remote_copy(
-            region, region, e_send.at[w, o], e_recv.at[w, o],
+            region, region, e_send.at[w, o - 1], e_recv.at[w, o - 1],
             device_id=(g, device, t), device_id_type=MESH)
 
     def give_own(w, early):
@@ -247,14 +255,24 @@
     def slot(stage):
         return 1 if stage == 1 else 0
 
+    HALF = R // 2
+
+    def window(stage):
+        return ds((stage - 2) * HALF, HALF) if stage > 1 else ds(0, R)
+
+    def block_of(stage, device):
+        if stage > 1:
+            return act.at[0, ds(device * R + (stage - 2) * HALF, HALF)]
+        return rows_of(slot(stage), device)
+
     def ag_x(stage, o):
-        region = rows_of(slot(stage), t)
-        return pltpu.make_async_remote_copy(
-            region, region, ag_x_send.at[stage, o], ag_x_recv.at[stage, o],
+        region = block_of(stage, t)
+        return pltpu.make_async_remote_copy(
+            region, region, ag_x_send.at[stage, o - 1], ag_x_recv.at[stage, o - 1],
             device_id=(g, f, x_peer(o) * CORES + c), device_id_type=MESH)
 
     def ag_c(stage, o, core):
-        region = rows_of(slot(stage), x_peer(X - o) * CORES + core)
+        region = block_of(stage, x_peer(X - o) * CORES + core)
         return pltpu.make_async_remote_copy(
             region, region, ag_c_send.at[stage, o], ag_c_recv.at[stage, o],
             device_id=partner, device_id_type=MESH)
@@ -265,9 +283,9 @@
         ag_c(stage, 0, c).start()
 
     def gather_forward_one(stage, o):
-        region = rows_of(slot(stage), x_peer(X - o) * CORES + c)
+        region = block_of(stage, x_peer(X - o) * CORES + c)
         pltpu.make_async_remote_copy(
-            region, region, ag_x_send.at[stage, o], ag_x_recv.at[stage, o],
+            region, region, ag_x_send.at[stage, o - 1], ag_x_recv.at[stage, o - 1],
             device_id=(g, f, t), device_id_type=MESH).wait_recv()
         ag_c(stage, o, c).start()
 
@@ -294,13 +312,14 @@
 
     def rs1(stage, q, j):
         return pltpu.make_async_remote_copy(
-            send1.at[q, j], recv1.at[q, j], rs1_send.at[stage, j], rs1_recv.at[stage, j],
+            send1.at[q, j, :, window(stage)], recv1.at[q, j, :, window(stage)],
+            rs1_send.at[stage, j], rs1_recv.at[stage, j],
             device_id=partner, device_id_type=MESH)
 
     def rs2(stage, q, j, o):
         return pltpu.make_async_remote_copy(
-            send1.at[q, j, o], recv2.at[q, j, o], rs2_send.at[stage, j, o],
-            rs2_recv.at[stage, j, o],
+            send1.at[q, j, o, window(stage)], recv2.at[q, j, o, window(stage)],
+            rs2_send.at[stage, j, o - 1], rs2_recv.at[stage, j, o - 1],
             device_id=(g, f, x_peer(o) * CORES + c), device_id_type=MESH)
 
     def give_back(j, device):
@@ -308,13 +327,15 @@
             send1.at[1, j, 0], recv2.at[0, j, 0], ret_send.at[j], ret_recv.at[j],
             device_id=(g, device, t), device_id_type=MESH)
 
-    def partial_rows(w, width, q, j, device):
+    def partial_rows(stage, w, width, q, j, device):
         r = shards[w].shape[0]
-        return dot(values[q, ds(device * R, R), :width], bufs[w][ds(j * r, r), :])
+        rows = (ds(device * R + (stage - 2) * HALF, HALF) if stage > 1 else ds(device * R, R))
+        return dot(values[q, rows, :width], bufs[w][ds(j * r, r), :])
 
     def sum_send(stage, q, w, width, j):
         def one(o, _):
-            send1[q, j, o] = partial_rows(w, width, q, j, o * CORES + (1 - c)).astype(bf16)
+            send1[q, j, o, window(stage)] = partial_rows(
+                stage, w, width, q, j, o * CORES + (1 - c)).astype(bf16)
             return 0
         lax.fori_loop(0, X, one, 0)
         rs1(stage, q, j).start()
@@ -323,18 +344,18 @@
         rs1(stage, q, j).wait()
         def pair(o):
             peer = x_peer(o)
-            return (partial_rows(w, width, q, j, peer * CORES + c)
-                    + recv1[q, j, peer].astype(f32))
+            return (partial_rows(stage, w, width, q, j, peer * CORES + c)
+                    + recv1[q, j, peer, window(stage)].astype(f32))
         for o in range(1, X):
-            send1[q, j, o] = pair(o).astype(bf16)
+            send1[q, j, o, window(stage)] = pair(o).astype(bf16)
             rs2(stage, q, j, o).start()
-        acc[q, :, ds(j * cols, cols)] = pair(0)
+        acc[q, window(stage), ds(j * cols, cols)] = pair(0)
 
     def sum_finish(stage, q, j):
-        block = acc[q, :, ds(j * cols, cols)]
+        block = acc[q, window(stage), ds(j * cols, cols)]
         for o in range(1, X):
             rs2(stage, q, j, o).wait_recv()
-            block += recv2[q, j, o].astype(f32)
+            block += recv2[q, j, o, window(stage)].astype(f32)
         return block
 
     def sum_drain(stage, q):
@@ -344,7 +365,7 @@
             return 0
         lax.fori_loop(0, F, one, 0)
 
-    RT = min(32, R)
+    RT = min(32, R // 2)
 
     def norm_in():
         def one(i, _):
@@ -354,21 +375,44 @@
             return 0
         lax.fori_loop(0, R // RT, one, 0)
 
-    def norm_mid():
+    def norm_mid(part):
         def one(i, _):
             rows = ds(i * RT, RT)
             mid = tokens[rows].astype(f32) + rms(total[rows]) * gains[1:2]
             after[rows] = mid
             act[0, ds(t * R + i * RT, RT)] = (rms(mid) * gains[2:3]).astype(bf16)
             return 0
-        lax.fori_loop(0, R // RT, one, 0)
-
-    def norm_out():
+        count = HALF // RT
+        lax.fori_loop(part * count, (part + 1) * count, one, 0)
+
+    PARTS = 4
+
+    def out_copy(part):
+        rows = ds(part * (R // PARTS), R // PARTS)
+        return pltpu.make_async_copy(rows_out.at[rows], out.at[rows], out_sem.at[part])
+
+    def norm_out(half):
+        tall = min(RT, R // PARTS)
+
         def one(i, _):
-            rows = ds(i * RT, RT)
-            out[rows] = (after[rows] + rms(total[rows]) * gains[3:4]).astype(bf16)
-            return 0
-        lax.fori_loop(0, R // RT, one, 0)
+            rows = ds(i * tall, tall)
+            rows_out[rows] = (after[rows] + rms(total[rows]) * gains[3:4]).astype(bf16)
+            return 0
+        count = R // PARTS // tall
+        for part in range(half * PARTS // 2, (half + 1) * PARTS // 2):
+            lax.fori_loop(part * count, (part + 1) * count, one, 0)
+            out_copy(part).start()
+
+    def tables():
+        step = fine.shape[1]
+
+        def one(i, _):
+            rows = ds(i * step, step)
+            far_cos, far_sin = coarse[0, pl.ds(i, 1)], coarse[1, pl.ds(i, 1)]
+            cosine[rows] = far_cos * fine[0] - far_sin * fine[1]
+            sine[rows] = far_sin * fine[0] + far_cos * fine[1]
+            return 0
+        lax.fori_loop(0, L // step, one, 0)
 
     def tiles(width, tile, body):
         across = width // tile
@@ -424,18 +468,18 @@
                 silu(swish) * values[q, rows, cols].astype(f32)).astype(bf16)
         tiles(heads * VD, VD, body)
 
-    def hidden_units(device):
+    def hidden_units(device, part):
         tile = math.gcd(FH, 256)
 
         def one(i, _):
-            rows, cols = ds(device * R, R), ds(i * tile, tile)
+            rows, cols = ds(device * R + part * HALF, HALF), ds(i * tile, tile)
             up = dot(act[0, rows], bufs[WU][:, cols])
             gate = dot(act[0, rows], bufs[WG][:, cols])
             values[0, rows, cols] = (silu(gate) * up).astype(bf16)
             return 0
         lax.fori_loop(0, FH // tile, one, 0)
 
-    def sums(stage, q, w, width, items, who=None, first=None):
+    def sums(stage, q, w, width, items, who=None, first=None, wait=True):
         def condition(k, d):
             if k == 0:
                 return who
@@ -444,7 +488,7 @@
         for n in range(len(items) + 1):
             if n < len(items):
                 k, d = items[n]
-                if k:
+                if k and wait:
                     arrived_from(w, k, d, first)
                 when(condition(k, d), lambda k=k, d=d: sum_send(stage, q, w, width, source(d, k)))
             if n > 0:
@@ -457,7 +501,7 @@
 
     def finish_own(stage):
         def one(j, _):
-            acc[0, :, ds(j * cols, cols)] = sum_finish(stage, 0, j)
+            acc[0, window(stage), ds(j * cols, cols)] = sum_finish(stage, 0, j)
             return 0
         lax.fori_loop(0, F, one, 0)
 
@@ -491,6 +535,7 @@
     for w in (WG, WU, WD):
         local_copy(w).wait()
         give_own(w, True)
+    pl.when(not_end)(tables)
     comm(WQ, 1, 0)
     comm(WQ, 1, 1)
     rest(WQ, 0)
@@ -586,8 +631,8 @@
     rest(WG, 1)
     comm(WD, 1, 1)
     sums(1, 1, WM, heads * VD, far, is_host, is_host)
+    pl.when(is_host)(lambda: finish_client(source(1, 1)))
     sums(0, 0, WM, heads * VD, near[2:] + far, not_end, guest)
-    pl.when(is_host)(lambda: finish_client(source(1, 1)))
     for k in range(2, F):
         along_z(WU, k, 0, not_end, False)
         along_y(WU, k, 0, not_end)
@@ -608,36 +653,40 @@
     def _():
         client_copy(host).wait_send()
         take_back()
-        norm_mid()
-        gather_start(2)
+        for part in range(2):
+            norm_mid(part)
+            gather_start(2 + part)
 
     @pl.when(not_end)
     def _():
         finish_own(0)
         sum_drain(0, 0)
-        norm_mid()
-        gather_start(2)
+        for part in range(2):
+            norm_mid(part)
+            gather_start(2 + part)
     for k in range(3, F):
         comm(WU, k, 0, is_end)
         comm(WD, k, 0, is_end)
     arrived(WG)
     arrived(WU)
-    ag_c(2, 0, 1 - c).wait_recv()
-    hidden_units(t)
-    hidden_units(x * CORES + 1 - c)
-    for o in range(1, X):
-        gather_forward_one(2, o)
-        hidden_units(x_peer(X - o) * CORES + c)
-    for o in range(1, X):
-        ag_c(2, o, 1 - c).wait_recv()
-        hidden_units(x_peer(X - o) * CORES + 1 - c)
-    sums(2, 0, WD, FH, near)
-    for k, d in far:
-        sums(2, 0, WD, FH, [(k, d)])
-    finish_own(2)
-    norm_out()
-    gather_drain(2)
-    sum_drain(2, 0)
+    for part in range(2):
+        hidden_units(t, part)
+        ag_c(2 + part, 0, 1 - c).wait_recv()
+        hidden_units(x * CORES + 1 - c, part)
+    for part in range(2):
+        stage = 2 + part
+        for o in range(1, X):
+            gather_forward_one(stage, o)
+            hidden_units(x_peer(X - o) * CORES + c, part)
+        for o in range(1, X):
+            ag_c(stage, o, 1 - c).wait_recv()
+            hidden_units(x_peer(X - o) * CORES + 1 - c, part)
+        sums(stage, 0, WD, FH, near + far, wait=part == 0)
+    for part in range(2):
+        finish_own(2 + part)
+        norm_out(part)
+        gather_drain(2 + part)
+        sum_drain(2 + part, 0)
 
     @pl.when(is_host)
     def _():
@@ -650,6 +699,8 @@
         lax.fori_loop(0, F, one, 0)
     for w in range(8):
         drain(w)
+    for part in range(PARTS):
+        out_copy(part).wait()
 
 
 def per_device(tokens, norm_gains, *weights):
@@ -659,9 +710,13 @@
     L = R * T
     query, _, value, _, mixer, gate, _, down = weights
     qk_width, v_width, hidden = query.shape[1], value.shape[1], gate.shape[1]
-    positions = jnp.arange(L, dtype=f32)
-    frequency = 10000.0 ** (-jnp.linspace(0.0, 1.0, QK // 2, dtype=f32))
-    angles = positions[:, None] * frequency[None, :]
+    step = math.gcd(L, 32)
+    frequency = np.float32(10000.0) ** (-np.linspace(0.0, 1.0, QK // 2, dtype=np.float32))
+    frequency = frequency.astype(np.float64)
+
+    def table(positions):
+        angles = positions[:, None] * frequency[None, :]
+        return jnp.asarray(np.stack([np.cos(angles), np.sin(angles)]).astype(np.float32))
     vmem = pl.BlockSpec(memory_space=pltpu.VMEM)
     anywhere = pl.BlockSpec(memory_space=pl.ANY)
     DMA = pltpu.SemaphoreType.DMA
@@ -676,22 +731,26 @@
         pltpu.VMEM((2, F, X, R, cols), bf16),
         pltpu.VMEM((2, F, X, R, cols), bf16),
         pltpu.VMEM((2, F, X, R, cols), bf16),
+        pltpu.VMEM((L, QK // 2), f32),
+        pltpu.VMEM((L, QK // 2), f32),
+        pltpu.VMEM((R, D), bf16),
         DMA((8,)),
-        DMA((2, 8, F)), DMA((2, 8, F)), DMA((2, 8, F, G)), DMA((2, 8, F, G)),
-        DMA((8, G)), DMA((8, G)),
-        DMA((3, X)), DMA((3, X)), DMA((3, X)), DMA((3, X)),
-        DMA((3, F)), DMA((3, F)), DMA((3, F, X)), DMA((3, F, X)),
-        DMA((2,)), DMA((F,)), DMA((F,)),
+        DMA((8, F + (F - 1) // 2)), DMA((8, F)),
+        DMA((8, F - 1 + (F - 1) // 2, G - 1)), DMA((8, F - 1 + (F - 1) // 2, G - 1)),
+        DMA((8, G - 1)), DMA((8, G - 1)),
+        DMA((4, X - 1)), DMA((4, X - 1)), DMA((4, X)), DMA((4, X)),
+        DMA((4, F)), DMA((4, F)), DMA((4, F, X - 1)), DMA((4, F, X - 1)),
+        DMA((2,)), DMA((F,)), DMA((F,)), DMA((4,)),
     ]
     return pl.pallas_call(
         functools.partial(layer, G, F, T),
         out_shape=jax.ShapeDtypeStruct((R, D), bf16),
         in_specs=[vmem] * 4 + [anywhere] * 8,
-        out_specs=vmem,
+        out_specs=anywhere,
         scratch_shapes=scratch,
         compiler_params=pltpu.CompilerParams(
             collective_id=0, has_side_effects=True, vmem_limit_bytes=67043328),
-    )(tokens, norm_gains, jnp.cos(angles), jnp.sin(angles), *weights)
+    )(tokens, norm_gains, table(np.arange(0.0, L, step)), table(np.arange(0.0, step)), *weights)
 
 
 def solution(mesh):

time: 242 us -> 227 us (0.938)
  Pallas kernels: 233 us -> 221 us
  other arithmetic: 2.9 us -> 0 us
    pallas_call x1, Pallas kernels: 233 us -> 221 us  [per_device(): pl.pallas_call(functools.partial(layer, G, F, T), out_shape=jax.ShapeDtyp...]
    sin x1 -> x0, other arithmetic: 2.8 us -> none  [per_device(): jnp.sin(angles)]
where the time goes in v3:
time: 227 us; the launch traced here: 223 us
  Pallas kernels  221 us (97%)
  local copies, waits for them, and re-layouts  2.3 us (1%)
    pallas_call x1, Pallas kernels, per_device(): pl.pallas_call(functools.partial(layer, G, F, T), out_shape=jax.ShapeDtyp...  221 us

profile of v3, /device:TPU:24, one launch (start us, length us, event | category | flops | bytes accessed | tf_op | source)
XLA Modules:
  0.0 223.3 jit_solution(3552056498995874036)
XLA Ops:
  0.0 221.0 %shard_map.118 = bf16[256,2048]{1,0:T(8,128)(2,1)} custom-call(bf16[256,2048]{1,0:T(8,128)(2,1)} %refs_0_.1, f32[4,2048]{1,0:T(4,128)} %refs_1_.1, f32[2,32,128]{2,1,0:T(8,128)} %constant.4.clone.refs_2_, f32[2,32,128]{2,1,0:T(8,128)} %constant.5.clone.refs_3_, bf16[512,512]{1,0:T(8,128)(2,1)} %refs_4_.1, bf16[512,512]{1,0:T(8,128)(2,1)} %refs_5_.1, ...), custom_call_target="tpu_custom_call" | custom-call | tf_op jit(solution)/shard_map/pallas_call | solution.py:745
  221.0 2.3 %copy.14 = bf16[256,2048]{1,0:T(8,128)(2,1)} copy(bf16[256,2048]{1,0:T(8,128)(2,1)} %shard_map.118) | data formatting | bytes 2097152

commit v4 on v3

--- a/solution.py
+++ b/solution.py
@@ -417,10 +417,12 @@
     def tiles(width, tile, body):
         across = width // tile
 
+        tall = min(512, L)
+
         def one(i, _):
-            body(ds((i // across) * TM, TM), ds((i % across) * tile, tile))
-            return 0
-        lax.fori_loop(0, (L // TM) * across, one, 0)
+            body(ds((i // across) * tall, tall), ds((i % across) * tile, tile))
+            return 0
+        lax.fori_loop(0, (L // tall) * across, one, 0)
 
     def rotary(q, w, into, scale):
         def body(rows, cols):
@@ -613,17 +615,17 @@
     along_z(WD, 1, 0)
     along_y(WD, 1, 0, is_end)
     pl.when(not_end)(lambda: project_swish(0))
-    along_y(WG, 1, 0, not_end)
     pl.when(not_end)(lambda: gather_drain(0))
+    sums(0, 0, WM, heads * VD, near[:1], not_end, guest)
 
     @pl.when(is_host)
     def _():
         finish_client(f)
         finish_client(source(0, 1))
-    sums(0, 0, WM, heads * VD, near[:1], not_end, guest)
     comm(WU, 1, 1)
     rest(WM, 0)
     rest(WM, 1)
+    along_y(WG, 1, 0, not_end)
     sums(1, 1, WM, heads * VD, near[2:], is_host, is_host)
     along_y(WU, 1, 0, not_end)
     sums(0, 0, WM, heads * VD, near[1:2], not_end, guest)

time: 227 us -> 223 us (0.982)
    pallas_call x1, Pallas kernels: 221 us -> 219 us  [per_device(): pl.pallas_call(functools.partial(layer, G, F, T), out_shape=jax.ShapeDtyp...]
where the time goes in v4:
time: 223 us; the launch traced here: 221 us
  Pallas kernels  219 us (98%)
  local copies, waits for them, and re-layouts  2.3 us (1%)
    pallas_call x1, Pallas kernels, per_device(): pl.pallas_call(functools.partial(layer, G, F, T), out_shape=jax.ShapeDtyp...  219 us

profile of v4, /device:TPU:24, one launch (start us, length us, event | category | flops | bytes accessed | tf_op | source)
XLA Modules:
  0.0 220.9 jit_solution(6488420000967228973)
XLA Ops:
  0.0 218.6 %shard_map.118 = bf16[256,2048]{1,0:T(8,128)(2,1)} custom-call(bf16[256,2048]{1,0:T(8,128)(2,1)} %refs_0_.1, f32[4,2048]{1,0:T(4,128)} %refs_1_.1, f32[2,32,128]{2,1,0:T(8,128)} %constant.4.clone.refs_2_, f32[2,32,128]{2,1,0:T(8,128)} %constant.5.clone.refs_3_, bf16[512,512]{1,0:T(8,128)(2,1)} %refs_4_.1, bf16[512,512]{1,0:T(8,128)(2,1)} %refs_5_.1, ...), custom_call_target="tpu_custom_call" | custom-call | tf_op jit(solution)/shard_map/pallas_call | solution.py:747
  218.6 2.3 %copy.14 = bf16[256,2048]{1,0:T(8,128)(2,1)} copy(bf16[256,2048]{1,0:T(8,128)(2,1)} %shard_map.118) | data formatting | bytes 2097152
